TPU v7x, 32 devices: a whole 2x2x4 slice. The times are simulated.
32 devices in a mesh: ep: 4 (over y, x), tp: 8 (over z, core).
Axes of the slice: x: 2, y: 2, z: 4, core: 2. Of those that a mesh axis runs over, the one named last changes fastest.
Arguments:
- hidden: bfloat16 [64, 2048], P('ep'), may hold values from -6 to 6
- attn_gain: float32 [2048], replicated, may hold values from 0.1 to 1.9
- query_weight: bfloat16 [2048, 1024], P(None, 'tp'), may hold values from -0.125 to 0.125
- rotary_weight: bfloat16 [2048, 512], P(None, 'tp'), may hold values from -0.125 to 0.125
- key_up: bfloat16 [16, 64, 512], P('tp'), may hold values from -0.75 to 0.75
- cache_latent: bfloat16 [64, 4096, 512], P(('ep', 'tp'))
- cache_rotary: bfloat16 [64, 32, 4096], P(('ep', 'tp')), may hold values from -6 to 6
- lengths: int32 [64], P(('ep', 'tp')), may hold values from 1 to 4096, as said below
- value_up: bfloat16 [16, 512, 64], P('tp'), may hold values from -0.25 to 0.25
- out_weight: bfloat16 [1024, 2048], P('tp'), may hold values from -0.1875 to 0.1875
- mixed_gain: float32 [2048], replicated, may hold values from 0.1 to 1.9
- moe_gain: float32 [2048], replicated, may hold values from 0.1 to 1.9
- expert_ids: int32 [64, 2], replicated, may hold values from 0 to 3, all different within a row; in each aligned block of 16 rows (0 to 15, 16 to 31, ...) at most 16 rows name the same one
- route_logits: float32 [64, 2], replicated, may hold values from -6 to 6
- gate_weight: bfloat16 [4, 2048, 7168], P('ep', None, 'tp'), may hold values from -0.125 to 0.125
- up_weight: bfloat16 [4, 2048, 7168], P('ep', None, 'tp'), may hold values from -0.125 to 0.125
- down_weight: bfloat16 [4, 7168, 2048], P('ep', 'tp'), may hold values from -0.0625 to 0.0625
- final_gain: float32 [2048], replicated, may hold values from 0.1 to 1.9
Outputs:
- layer_out: bfloat16 [64, 2048], P(('ep', 'tp'))
Inputs may be any that keep to these rules, and one draw needn't show every extreme that they name: `lengths`: some sequence has exactly 4096 filled positions. `expert_ids`: within each aligned block of 16 rows no expert is named more than 16 times, a bound that some block reaches.
All inputs are finite; a program needn't handle non-finite values.
Results may differ from a plain program's by a relative error of at most 0.023.
The roundings to bfloat16 on the way count: a program that leaves them out, or rounds other values in their place, can miss the bound.
Values may be sent and summed in bfloat16 or wider, within the bound.
A program may use at most 64 MiB of HBM per device.

v0:
```python
import jax
import jax.numpy as jnp
from jax import lax
from jax.sharding import PartitionSpec as P

EPSILON = 1e-06


def norm_rows(values, gain_vector):
    values = values.astype(jnp.float32)
    factor = lax.rsqrt(jnp.mean(values * values, axis=-1, keepdims=True) + EPSILON)
    return values * factor * gain_vector


def rotate(values, position):
    half_width = values.shape[-1] // 2
    inverse = 10000.0 ** (-jnp.arange(half_width, dtype=jnp.float32) / half_width)
    angles = position.astype(jnp.float32)[:, None, None] * inverse
    cosine = jnp.cos(angles)
    sine_part = jnp.sin(angles)
    first_half = values[..., :half_width]
    second = values[..., half_width:]
    return jnp.concatenate(
        [first_half * cosine - second * sine_part, second * cosine + first_half * sine_part],
        axis=-1,
    )


def slot_tables(group_ids, group_probs, experts, capacity):
    row_count, top_count = group_ids.shape
    flat_ids = group_ids.reshape(-1)
    onehot = (flat_ids[:, None] == jnp.arange(experts, dtype=jnp.int32)[None, :]).astype(jnp.int32)
    earlier = jnp.cumsum(onehot, axis=0) - onehot
    slot_index = jnp.sum(earlier * onehot, axis=1)
    target = flat_ids * capacity + slot_index
    source = jnp.arange(row_count * top_count, dtype=jnp.int32) // top_count
    slot_rows = jnp.full((experts * capacity,), row_count, jnp.int32).at[target].set(source)
    slot_gates = (
        jnp.zeros((experts * capacity,), jnp.float32).at[target].set(group_probs.reshape(-1))
    )
    return (slot_rows, slot_gates)


def expert_rows(picked, gate_weight, up_weight, down_weight):
    gate_part = jnp.einsum("jnd,jdf->jnf", picked, gate_weight, preferred_element_type=jnp.float32)
    up_part = jnp.einsum("jnd,jdf->jnf", picked, up_weight, preferred_element_type=jnp.float32)
    act = (jax.nn.silu(gate_part) * up_part).astype(jnp.bfloat16)
    return jnp.einsum("jnf,jfd->jnd", act, down_weight, preferred_element_type=jnp.float32)


def body(
    hidden,
    attn_gain,
    query_weight,
    rotary_weight,
    key_up,
    cache_latent,
    cache_rotary,
    lengths,
    value_up,
    out_weight,
    mixed_gain,
    moe_gain,
    expert_ids,
    route_logits,
    gate_weight,
    up_weight,
    down_weight,
    final_gain,
):
    group_rows, features = hidden.shape
    local_heads, nope_width, latent_width = key_up.shape
    rotary_width = rotary_weight.shape[1] // local_heads
    own_rows = cache_latent.shape[0]
    groups = lax.axis_size("ep")
    own_start = lax.axis_index("tp") * own_rows
    normed_in = norm_rows(hidden, attn_gain).astype(jnp.bfloat16)
    query_nope = jnp.dot(normed_in, query_weight, preferred_element_type=jnp.float32).astype(
        jnp.bfloat16
    )
    query_nope = query_nope.reshape(group_rows, local_heads, nope_width)
    query_pe = jnp.dot(normed_in, rotary_weight, preferred_element_type=jnp.float32).astype(
        jnp.bfloat16
    )
    query_pe = query_pe.reshape(group_rows, local_heads, rotary_width)
    query_latent = jnp.einsum(
        "shn,hnc->shc", query_nope, key_up, preferred_element_type=jnp.float32
    ).astype(jnp.bfloat16)
    query_latent, query_pe = (
        lax.all_to_all(query_latent, "tp", split_axis=0, concat_axis=1, tiled=True),
        lax.all_to_all(query_pe, "tp", split_axis=0, concat_axis=1, tiled=True),
    )
    query_rot = rotate(query_pe.astype(jnp.float32), lengths - 1).astype(jnp.bfloat16)
    score_scale = (nope_width + rotary_width) ** (-0.5)
    scores = jnp.einsum(
        "bhc,bpc->bhp", query_latent, cache_latent, preferred_element_type=jnp.float32
    )
    scores = scores + jnp.einsum(
        "bhr,brp->bhp", query_rot, cache_rotary, preferred_element_type=jnp.float32
    )
    scores = scores * score_scale
    visible = (
        jnp.arange(cache_latent.shape[1], dtype=jnp.int32)[None, None, :] < lengths[:, None, None]
    )
    scores = jnp.where(visible, scores, -jnp.inf)
    highest = jnp.max(scores, axis=-1, keepdims=True)
    weights = jnp.exp(scores - highest)
    probs = (weights / jnp.sum(weights, axis=-1, keepdims=True)).astype(jnp.bfloat16)
    out_latent = jnp.einsum(
        "bhp,bpc->bhc", probs, cache_latent, preferred_element_type=jnp.float32
    ).astype(jnp.bfloat16)
    out_latent = lax.all_to_all(out_latent, "tp", split_axis=1, concat_axis=0, tiled=True)
    head_out = jnp.einsum(
        "shc,hcv->shv", out_latent, value_up, preferred_element_type=jnp.float32
    ).astype(jnp.bfloat16)
    head_terms = jnp.dot(
        head_out.reshape(group_rows, -1), out_weight, preferred_element_type=jnp.float32
    )
    attended = lax.psum(head_terms.astype(jnp.bfloat16), "tp")
    mixed_group = (hidden.astype(jnp.float32) + norm_rows(attended, mixed_gain)).astype(
        jnp.bfloat16
    )
    normed = norm_rows(mixed_group, moe_gain).astype(jnp.bfloat16)
    mixed_rows = lax.dynamic_slice_in_dim(mixed_group, own_start, own_rows, 0)
    local_experts = gate_weight.shape[0]
    experts_all = local_experts * groups
    top_count = expert_ids.shape[1]
    capacity = 2 * group_rows * top_count // experts_all
    gate_probs = jax.nn.softmax(route_logits, axis=-1)
    gathered = lax.all_gather(normed, "ep", axis=0, tiled=True)
    all_count = gathered.shape[0]

    def tables_for(group_ids, group_probs):
        return slot_tables(group_ids, group_probs, experts_all, capacity)

    slot_rows, slot_gates = jax.vmap(tables_for)(
        expert_ids.reshape(groups, group_rows, top_count),
        gate_probs.reshape(groups, group_rows, top_count),
    )
    offsets = jnp.arange(groups, dtype=jnp.int32)[:, None] * group_rows
    global_rows = jnp.where(slot_rows < group_rows, slot_rows + offsets, all_count)
    first_expert = lax.axis_index("ep") * local_experts
    my_rows = lax.dynamic_slice_in_dim(
        global_rows.reshape(groups, experts_all, capacity), first_expert, local_experts, 1
    )
    my_gates = lax.dynamic_slice_in_dim(
        slot_gates.reshape(groups, experts_all, capacity), first_expert, local_experts, 1
    )
    my_rows = my_rows.transpose(1, 0, 2).reshape(local_experts, groups * capacity)
    my_gates = my_gates.transpose(1, 0, 2).reshape(local_experts, groups * capacity)
    padded_all = jnp.concatenate([gathered, jnp.zeros((1, features), jnp.bfloat16)], axis=0)
    result = (
        expert_rows(padded_all[my_rows], gate_weight, up_weight, down_weight) * my_gates[..., None]
    )
    spread = (
        jnp.zeros((all_count + 1, features), jnp.float32)
        .at[my_rows.reshape(-1)]
        .add(result.reshape(-1, features))
    )
    routed = lax.psum_scatter(spread[:all_count], ("ep", "tp"), scatter_dimension=0, tiled=True)
    routed = routed.astype(jnp.bfloat16)
    return (mixed_rows.astype(jnp.float32) + norm_rows(routed, final_gain)).astype(jnp.bfloat16)


def solution(mesh):
    placed = (
        P("ep", None),
        P(),
        P(None, "tp"),
        P(None, "tp"),
        P("tp", None, None),
        P(("ep", "tp"), None, None),
        P(("ep", "tp"), None, None),
        P(("ep", "tp")),
        P("tp", None, None),
        P("tp", None),
        P(),
        P(),
        P(),
        P(),
        P("ep", None, "tp"),
        P("ep", None, "tp"),
        P("ep", "tp", None),
        P(),
    )
    return jax.shard_map(
        body, mesh=mesh, in_specs=placed, out_specs=P(("ep", "tp"), None), check_vma=False
    )
```

profile of v0, /device:TPU:0, one launch (start us, length us, event | category | flops | bytes accessed | tf_op | source)
XLA Modules:
  0.0 193.6 jit_solution(2101767761909809505)
XLA Ops:
  6.6 1.1 fusion.37
  7.6 1.2 convolution_convert_fusion.4
  8.9 0.7 reshape.273
  9.6 6.4 %all-to-all-start.1 = ((bf16[16,2,32]{2,1,0:T(2,128)(2,1)}), bf16[16,2,32]{2,1,0:T(2,128)(2,1)S(1)}, u32[]{:S(2)}, u32[]{:S(2)}) async-start(bf16[16,2,32]{2,1,0:T(2,128)(2,1)} %reshape.273), calls=%async_computation.1 | async-start | bytes 16384 | tf_op jit(solution)/shard_map/all_to_all | solution.py:91
  15.9 0.7 add_convert_fusion.1
  16.6 0.7 iota_compare_fusion.1
  17.3 0.8 copy.46
  18.1 0.7 broadcast_multiply_fusion
  18.8 0.1 eq.15
  18.9 0.1 fusion.42
  19.1 0.2 select_reduce_fusion
  19.3 0.1 copy.45
  19.4 0.1 mul.205
  19.6 0.1 reshape.301
  19.7 6.4 %scatter_fusion = s32[4,64]{1,0:T(4,128)S(1)} fusion(s32[4,64]{1,0:T(4,128)S(1)} %broadcast.223, s32[128]{0:T(128)S(1)} %reshape.299, s32[128]{0:T(128)S(1)} %reshape.301), kind=kCustom, calls=%fused_computation.2 | custom fusion | bytes 2560 | tf_op jit(solution)/shard_map/vmap()/scatter | solution.py:37
  26.1 0.1 reshape.275
  26.2 0.1 reshape_transpose.3
  26.4 0.2 convolution_convert_fusion.5
  26.7 0.1 reshape.272
  26.8 0.1 multiply_cosine_fusion
  26.9 0.1 fusion.20
  27.1 0.6 copy.39
  27.7 0.1 copy.48
  27.8 0.1 reshape.307
  28.0 6.4 %scatter_fusion.1 = f32[4,64]{1,0:T(4,128)S(1)} fusion(f32[4,64]{1,0:T(4,128)S(1)} %broadcast_in_dim.26, s32[128]{0:T(128)S(1)} %reshape.299, f32[128]{0:T(128)S(1)} %reshape.307), kind=kCustom, calls=%fused_computation.3 | custom fusion | bytes 2560 | tf_op jit(solution)/shard_map/vmap()/scatter | solution.py:39
  34.5 5.1 %all-to-all-start = ((bf16[16,2,512]{2,1,0:T(2,128)(2,1)}), bf16[16,2,512]{2,1,0:T(2,128)(2,1)S(1)}, u32[]{:S(2)}, u32[]{:S(2)}) async-start(bf16[16,2,512]{2,1,0:T(2,128)(2,1)} %copy.39), calls=%async_computation | async-start | bytes 65536 | tf_op jit(solution)/shard_map/all_to_all | solution.py:90
  39.6 5.7 %all-to-all-done = bf16[16,2,512]{2,1,0:T(2,128)(2,1)S(1)} async-done(((bf16[16,2,512]{2,1,0:T(2,128)(2,1)}), bf16[16,2,512]{2,1,0:T(2,128)(2,1)S(1)}, u32[]{:S(2)}, u32[]{:S(2)}) %all-to-all-start) | async-done | bytes 32800 | tf_op jit(solution)/shard_map/all_to_all | solution.py:90
  45.3 5.7 %fusion.66 = f32[2,16,4096]{2,1,0:T(8,128)S(1)} fusion(bf16[2,16,512]{2,1,0:T(8,128)(2,1)S(1)} %all_to_all.36, bf16[2,4096,512]{2,1,0:T(8,128)(2,1)} %param.23), kind=kOutput, calls=%fused_computation.111 | convolution fusion | flops 134217728 | bytes 8945664 | tf_op jit(solution)/shard_map/bhc,bpc->bhp/dot_general | solution.py:95
  51.0 0.3 fusion.3
  51.3 0.3 fusion.65
  51.6 4.7 %convolution_convert_fusion.1 = bf16[2,16,512]{2,1,0:T(8,128)(2,1)S(1)} fusion(bf16[2,4096,512]{2,1,0:T(8,128)(2,1)} %param.23, f32[2,16]{1,0:T(2,128)S(1)} %fusion.65, f32[2,16,4096]{2,1,0:T(8,128)S(1)} %fusion.3), kind=kOutput, calls=%fused_computation.20 | convolution fusion | flops 134631456 | bytes 8945792 | tf_op jit(solution)/shard_map/bhp,bpc->bhc/dot_general | solution.py:109
  56.3 0.6 copy.42
  57.0 3.3 %all-to-all-start.2 = ((bf16[2,16,512]{2,0,1:T(2,128)(2,1)}), bf16[2,16,512]{2,0,1:T(2,128)(2,1)S(1)}, u32[]{:S(2)}, u32[]{:S(2)}) async-start(bf16[2,16,512]{2,0,1:T(2,128)(2,1)} %copy.42), calls=%async_computation.2 | async-start | bytes 65536 | tf_op jit(solution)/shard_map/all_to_all | solution.py:112
  60.4 5.6 %all-to-all-done.2 = bf16[2,16,512]{2,0,1:T(2,128)(2,1)S(1)} async-done(((bf16[2,16,512]{2,0,1:T(2,128)(2,1)}), bf16[2,16,512]{2,0,1:T(2,128)(2,1)S(1)}, u32[]{:S(2)}, u32[]{:S(2)}) %all-to-all-start.2) | async-done | bytes 32800 | tf_op jit(solution)/shard_map/all_to_all | solution.py:112
  66.1 0.1 fusion.21
  66.2 0.1 reshape.274
  66.3 0.8 convolution_convert_fusion
  67.3 53.0 %all-reduce.5.cloned.1.call-done = bf16[16,2048]{1,0:T(8,128)(2,1)} async-done(((bf16[16,2048]{1,0:T(8,128)(2,1)}), bf16[16,2048]{1,0:T(8,128)(2,1)}) %all-reduce.5.cloned.1.call-update) | async-done | bytes 65552 | tf_op jit(solution)/shard_map/psum | solution.py:119
  120.3 1.0 fusion.32
  121.3 1.1 fusion.34
  122.4 9.3 %all_gather.3 = bf16[64,2048]{1,0:T(8,128)(2,1)S(1)} all-gather(bf16[16,2048]{1,0:T(8,128)(2,1)S(1)} %fusion.36), channel_id=1, replica_groups=mesh['ep'=4,'tp'=8] {'ep'}, dimensions={0}, use_global_device_ids=true | all-gather | bytes 327680 | tf_op jit(solution)/shard_map/all_gather | solution.py:130
  131.7 0.7 gather_fusion
  132.5 2.7 %fusion.9 = f32[64,896]{1,0:T(8,128)S(1)} fusion(bf16[64,2048]{1,0:T(8,128)(2,1)S(1)} %gather_fusion, bf16[1,2048,896]{2,1,0:T(8,128)(2,1)} %param.32), kind=kOutput, calls=%fused_computation.14 | convolution fusion | flops 234881024 | bytes 4161536 | tf_op jit(solution)/shard_map/jnd,jdf->jnf/dot_general | solution.py:45
  135.2 4.7 %fusion.11 = f32[64,2048]{1,0:T(8,128)S(1)} fusion(bf16[1,896,2048]{2,1,0:T(8,128)(2,1)} %param.34, bf16[64,2048]{1,0:T(8,128)(2,1)S(1)} %gather_fusion, bf16[1,2048,896]{2,1,0:T(8,128)(2,1)} %param.33, f32[64]{0:T(128)S(1)} %mul.215, f32[64,896]{1,0:T(8,128)S(1)} %fusion.9), kind=kOutput, calls=%fused_computation.16 | convolution fusion | flops 470237184 | bytes 8356096 | tf_op jit(solution)/shard_map/jnf,jfd->jnd/dot_general | solution.py:48
  140.0 1.5 scatter_custom_fusion
  141.5 44.3 %all-reduce.6 = bf16[64,2048]{1,0:T(8,128)(2,1)S(1)} all-reduce(f32[64,2048]{1,0:T(8,128)S(1)} %slice.20), channel_id=2, replica_groups=mesh['ep'=4,'tp'=8] {'ep','tp'}, use_global_device_ids=true, to_apply=%region_13.14.clone | all-reduce | flops 131072 | bytes 786432
  185.9 0.1 fusion.43
  186.0 0.7 fusion.46
  (60 shorter events, 1.1 us)
Async XLA Ops:
  6.5 44.5 %copy-start = (bf16[2,32,4096]{2,1,0:T(8,128)(2,1)S(1)}, bf16[2,32,4096]{2,1,0:T(8,128)(2,1)}, u32[]{:S(2)}) copy-start(bf16[2,32,4096]{2,1,0:T(8,128)(2,1)} %param.24) | copy-start | bytes 1572868
  6.5 19.9 %copy-start.1 = (bf16[16,2048]{1,0:T(8,128)(2,1)S(1)}, bf16[16,2048]{1,0:T(8,128)(2,1)}, u32[]{:S(2)}) copy-start(bf16[16,2048]{1,0:T(8,128)(2,1)} %param.18) | copy-start | bytes 196612
  6.5 19.9 %copy-start.7 = (f32[2048]{0:T(1024)S(1)}, f32[2048]{0:T(1024)}, u32[]{:S(2)}) copy-start(f32[2048]{0:T(1024)} %param.19) | copy-start | bytes 24580
  6.5 19.9 %copy-start.3 = (bf16[2048,128]{1,0:T(8,128)(2,1)S(1)}, bf16[2048,128]{1,0:T(8,128)(2,1)}, u32[]{:S(2)}) copy-start(bf16[2048,128]{1,0:T(8,128)(2,1)} %param.20) | copy-start | bytes 1572868
  6.5 20.2 %copy-start.6 = (f32[64,2]{0,1:T(2,128)S(1)}, f32[64,2]{0,1:T(2,128)}, u32[]{:S(2)}) copy-start(f32[64,2]{0,1:T(2,128)} %param.31) | copy-start | bytes 1540
  6.5 20.4 %copy-start.4 = (bf16[2,64,512]{2,1,0:T(8,128)(2,1)S(1)}, bf16[2,64,512]{2,1,0:T(8,128)(2,1)}, u32[]{:S(2)}) copy-start(bf16[2,64,512]{2,1,0:T(8,128)(2,1)} %param.22) | copy-start | bytes 393220
  9.6 24.9 %all-to-all-start.1 = ((bf16[16,2,32]{2,1,0:T(2,128)(2,1)}), bf16[16,2,32]{2,1,0:T(2,128)(2,1)S(1)}, u32[]{:S(2)}, u32[]{:S(2)}) async-start(bf16[16,2,32]{2,1,0:T(2,128)(2,1)} %reshape.273), calls=%async_computation.1 | async-start | bytes 16384 | tf_op jit(solution)/shard_map/all_to_all | solution.py:91
  34.5 10.8 %all-to-all-start = ((bf16[16,2,512]{2,1,0:T(2,128)(2,1)}), bf16[16,2,512]{2,1,0:T(2,128)(2,1)S(1)}, u32[]{:S(2)}, u32[]{:S(2)}) async-start(bf16[16,2,512]{2,1,0:T(2,128)(2,1)} %copy.39), calls=%async_computation | async-start | bytes 65536 | tf_op jit(solution)/shard_map/all_to_all | solution.py:90
  51.6 14.5 %copy-start.5 = (bf16[2,512,64]{1,2,0:T(8,128)(2,1)S(1)}, bf16[2,512,64]{1,2,0:T(8,128)(2,1)}, u32[]{:S(2)}) copy-start(bf16[2,512,64]{1,2,0:T(8,128)(2,1)} %param.26) | copy-start | bytes 393220
  51.6 14.7 %copy-start.2 = (bf16[128,2048]{1,0:T(8,128)(2,1)S(1)}, bf16[128,2048]{1,0:T(8,128)(2,1)}, u32[]{:S(2)}) copy-start(bf16[128,2048]{1,0:T(8,128)(2,1)} %param.27) | copy-start | bytes 1572868
  51.6 69.7 %copy-start.8 = (f32[2048]{0:T(1024)S(1)}, f32[2048]{0:T(1024)}, u32[]{:S(2)}) copy-start(f32[2048]{0:T(1024)} %param.28) | copy-start | bytes 24580
  51.6 70.7 %copy-start.9 = (f32[2048]{0:T(1024)S(1)}, f32[2048]{0:T(1024)}, u32[]{:S(2)}) copy-start(f32[2048]{0:T(1024)} %param.29) | copy-start | bytes 24580
  57.0 9.0 %all-to-all-start.2 = ((bf16[2,16,512]{2,0,1:T(2,128)(2,1)}), bf16[2,16,512]{2,0,1:T(2,128)(2,1)S(1)}, u32[]{:S(2)}, u32[]{:S(2)}) async-start(bf16[2,16,512]{2,0,1:T(2,128)(2,1)} %copy.42), calls=%async_computation.2 | async-start | bytes 65536 | tf_op jit(solution)/shard_map/all_to_all | solution.py:112
  60.3 60.0 %all-reduce.5.cloned.1.call-start = ((), (), s32[]{:S(2)}) async-start(), calls=%async_computation.3 | async-start | bytes 131072 | tf_op jit(solution)/shard_map/psum | solution.py:119
  135.2 50.8 %copy-start.10 = (f32[2048]{0:T(1024)S(1)}, f32[2048]{0:T(1024)}, u32[]{:S(2)}) copy-start(f32[2048]{0:T(1024)} %param.35) | copy-start | bytes 24580
Sparse Core Ops, SparseCore 0:
  67.3 52.9 all-reduce.4
where the time goes:
time: 194 us
  waiting for transfers between devices  64.3 us (33%)
  blocking collectives  53.6 us (28%)
  matrix products  20.7 us (11%)
  local copies, waits for them, and re-layouts  17.8 us (9%)
  starting transfers between devices  14.8 us (8%)
  between operations  13.7 us (7%)
  other arithmetic  8.61 us (4%)
    psum x1, waiting for transfers between devices, body(): attended = lax.psum(head_terms.astype(jnp.bfloat16), 'tp')  53 us
    unnamed x1, blocking collectives  44.3 us
    all_gather x1, blocking collectives, body(): gathered = lax.all_gather(normed, 'ep', axis=0, tiled=True)  9.29 us
    scatter x2, local copies, waits for them, and re-layouts, slot_tables(): jnp.full((experts * capacity,), row_count, jnp.int32).at[target].set(source)  6.48 us
    scatter x1, local copies, waits for them, and re-layouts, slot_tables(): jnp.zeros((experts * capacity,), jnp.float32).at[target]  6.4 us
    all_to_all x1, starting transfers between devices, body(): lax.all_to_all(query_pe, 'tp', split_axis=0, concat_axis=1, tiled=True)  6.35 us
    dot_general x1, matrix products, body(): jnp.einsum('bhc,bpc->bhp', query_latent, cache_latent, preferred_element_...  5.66 us
    all_to_all x1, waiting for transfers between devices, body(): lax.all_to_all(query_latent, 'tp', split_axis=0, concat_axis=1, tiled=True)  5.65 us
  transfers between devices with their start and end apart: 4, of which 3 were waited for; matrix products, arithmetic and copies ran while one was open for 10% of the time, Pallas kernels for 0%

commit v1 on v0

--- a/solution.py
+++ b/solution.py
@@ -116,7 +116,7 @@
     head_terms = jnp.dot(
         head_out.reshape(group_rows, -1), out_weight, preferred_element_type=jnp.float32
     )
-    attended = lax.psum(head_terms.astype(jnp.bfloat16), "tp")
+    attended = jnp.sum(lax.all_gather(head_terms.astype(jnp.bfloat16), "tp"), axis=0)
     mixed_group = (hidden.astype(jnp.float32) + norm_rows(attended, mixed_gain)).astype(
         jnp.bfloat16
     )

time: 194 us -> 140 us (0.72)
  waiting for transfers between devices: 64.3 us -> 11.3 us
  blocking collectives: 53.6 us -> 67.9 us
  between operations: 13.7 us -> 0.3 us
    psum x1 -> x0, waiting for transfers between devices: 53 us -> none  [body(): attended = lax.psum(head_terms.astype(jnp.bfloat16), 'tp')]
    all_gather x0 -> x1, blocking collectives: none -> 15.1 us  [body(): lax.all_gather(head_terms.astype(jnp.bfloat16), 'tp')]
  transfers between devices with their start and end apart: 4 -> 3, of which waited for: 3 -> 2; matrix products, arithmetic and copies ran while one was open for 10% -> 13% of each run, Pallas kernels for 0% -> 0%
where the time goes in v1:
time: 140 us; the launch traced here: 139 us
  blocking collectives  67.9 us (49%)
  matrix products  20 us (14%)
  local copies, waits for them, and re-layouts  17.8 us (13%)
  starting transfers between devices  14.8 us (11%)
  waiting for transfers between devices  11.3 us (8%)
  other arithmetic  7 us (5%)
    unnamed x1, blocking collectives  43.9 us
    all_gather x1, blocking collectives, body(): lax.all_gather(head_terms.astype(jnp.bfloat16), 'tp')  15.1 us
    all_gather x1, blocking collectives, body(): gathered = lax.all_gather(normed, 'ep', axis=0, tiled=True)  8.99 us
    scatter x2, local copies, waits for them, and re-layouts, slot_tables(): jnp.full((experts * capacity,), row_count, jnp.int32).at[target].set(source)  6.48 us
    scatter x1, local copies, waits for them, and re-layouts, slot_tables(): jnp.zeros((experts * capacity,), jnp.float32).at[target]  6.4 us
    all_to_all x1, starting transfers between devices, body(): lax.all_to_all(query_pe, 'tp', split_axis=0, concat_axis=1, tiled=True)  6.36 us
    dot_general x1, matrix products, body(): jnp.einsum('bhc,bpc->bhp', query_latent, cache_latent, preferred_element_...  5.66 us
    all_to_all x1, waiting for transfers between devices, body(): lax.all_to_all(out_latent, 'tp', split_axis=1, concat_axis=0, tiled=True)  5.66 us
  transfers between devices with their start and end apart: 3, of which 2 were waited for; matrix products, arithmetic and copies ran while one was open for 13% of the time, Pallas kernels for 0%

profile of v1, /device:TPU:0, one launch (start us, length us, event | category | flops | bytes accessed | tf_op | source)
XLA Modules:
  0.0 139.2 jit_solution(10829412127954395125)
XLA Ops:
  0.0 1.1 fusion.37
  1.1 1.2 convolution_convert_fusion.4
  2.3 0.7 reshape.273
  3.0 6.4 %all-to-all-start.1 = ((bf16[16,2,32]{2,1,0:T(2,128)(2,1)}), bf16[16,2,32]{2,1,0:T(2,128)(2,1)S(1)}, u32[]{:S(2)}, u32[]{:S(2)}) async-start(bf16[16,2,32]{2,1,0:T(2,128)(2,1)} %reshape.273), calls=%async_computation.1 | async-start | bytes 16384 | tf_op jit(solution)/shard_map/all_to_all | solution.py:91
  9.4 0.7 add_convert_fusion.1
  10.1 0.7 iota_compare_fusion.1
  10.8 0.8 copy.46
  11.6 0.7 broadcast_multiply_fusion
  12.3 0.1 eq.15
  12.4 0.1 fusion.42
  12.5 0.2 select_reduce_fusion
  12.7 0.1 copy.45
  12.8 0.1 mul.205
  13.0 0.1 reshape.301
  13.1 6.4 %scatter_fusion = s32[4,64]{1,0:T(4,128)S(1)} fusion(s32[4,64]{1,0:T(4,128)S(1)} %broadcast.223, s32[128]{0:T(128)S(1)} %reshape.299, s32[128]{0:T(128)S(1)} %reshape.301), kind=kCustom, calls=%fused_computation.2 | custom fusion | bytes 2560 | tf_op jit(solution)/shard_map/vmap()/scatter | solution.py:37
  19.6 0.1 reshape.275
  19.7 0.1 reshape_transpose.3
  19.9 0.2 convolution_convert_fusion.5
  20.1 0.1 reshape.272
  20.3 0.1 copy.48
  20.4 0.1 reshape.307
  20.5 6.4 %scatter_fusion.1 = f32[4,64]{1,0:T(4,128)S(1)} fusion(f32[4,64]{1,0:T(4,128)S(1)} %broadcast_in_dim.26, s32[128]{0:T(128)S(1)} %reshape.299, f32[128]{0:T(128)S(1)} %reshape.307), kind=kCustom, calls=%fused_computation.3 | custom fusion | bytes 2560 | tf_op jit(solution)/shard_map/vmap()/scatter | solution.py:39
  27.0 0.1 multiply_cosine_fusion
  27.2 0.1 fusion.20
  27.3 0.6 copy.39
  28.0 5.1 %all-to-all-start = ((bf16[16,2,512]{2,1,0:T(2,128)(2,1)}), bf16[16,2,512]{2,1,0:T(2,128)(2,1)S(1)}, u32[]{:S(2)}, u32[]{:S(2)}) async-start(bf16[16,2,512]{2,1,0:T(2,128)(2,1)} %copy.39), calls=%async_computation | async-start | bytes 65536 | tf_op jit(solution)/shard_map/all_to_all | solution.py:90
  33.2 5.7 %all-to-all-done = bf16[16,2,512]{2,1,0:T(2,128)(2,1)S(1)} async-done(((bf16[16,2,512]{2,1,0:T(2,128)(2,1)}), bf16[16,2,512]{2,1,0:T(2,128)(2,1)S(1)}, u32[]{:S(2)}, u32[]{:S(2)}) %all-to-all-start) | async-done | bytes 32800 | tf_op jit(solution)/shard_map/all_to_all | solution.py:90
  38.9 5.7 %fusion.66 = f32[2,16,4096]{2,1,0:T(8,128)S(1)} fusion(bf16[2,16,512]{2,1,0:T(8,128)(2,1)S(1)} %all_to_all.36, bf16[2,4096,512]{2,1,0:T(8,128)(2,1)} %param.23), kind=kOutput, calls=%fused_computation.111 | convolution fusion | flops 134217728 | bytes 8945664 | tf_op jit(solution)/shard_map/bhc,bpc->bhp/dot_general | solution.py:95
  44.6 0.3 fusion.3
  44.9 0.3 fusion.65
  45.2 4.7 %convolution_convert_fusion.1 = bf16[2,16,512]{2,1,0:T(8,128)(2,1)S(1)} fusion(bf16[2,4096,512]{2,1,0:T(8,128)(2,1)} %param.23, f32[2,16]{1,0:T(2,128)S(1)} %fusion.65, f32[2,16,4096]{2,1,0:T(8,128)S(1)} %fusion.3), kind=kOutput, calls=%fused_computation.20 | convolution fusion | flops 134631456 | bytes 8945792 | tf_op jit(solution)/shard_map/bhp,bpc->bhc/dot_general | solution.py:109
  49.9 0.6 copy.42
  50.6 3.3 %all-to-all-start.2 = ((bf16[2,16,512]{2,0,1:T(2,128)(2,1)}), bf16[2,16,512]{2,0,1:T(2,128)(2,1)S(1)}, u32[]{:S(2)}, u32[]{:S(2)}) async-start(bf16[2,16,512]{2,0,1:T(2,128)(2,1)} %copy.42), calls=%async_computation.2 | async-start | bytes 65536 | tf_op jit(solution)/shard_map/all_to_all | solution.py:112
  53.9 5.7 %all-to-all-done.2 = bf16[2,16,512]{2,0,1:T(2,128)(2,1)S(1)} async-done(((bf16[2,16,512]{2,0,1:T(2,128)(2,1)}), bf16[2,16,512]{2,0,1:T(2,128)(2,1)S(1)}, u32[]{:S(2)}, u32[]{:S(2)}) %all-to-all-start.2) | async-done | bytes 32800 | tf_op jit(solution)/shard_map/all_to_all | solution.py:112
  59.6 0.1 fusion.21
  59.8 0.1 reshape.274
  59.9 0.2 convolution_convert_fusion
  60.1 15.1 %all-gather = bf16[128,2048]{1,0:T(8,128)(2,1)S(1)} all-gather(bf16[16,2048]{1,0:T(8,128)(2,1)S(1)} %convolution_convert_fusion), channel_id=2, replica_groups=mesh['ep'=4,'tp'=8] {'tp'}, dimensions={0}, use_global_device_ids=true | all-gather | bytes 589824 | tf_op jit(solution)/shard_map/all_gather | solution.py:119
  75.2 0.1 fusion.32
  75.3 0.2 fusion.34
  75.7 9.0 %all_gather.11 = bf16[64,2048]{1,0:T(8,128)(2,1)S(1)} all-gather(bf16[16,2048]{1,0:T(8,128)(2,1)S(1)} %fusion.36), channel_id=1, replica_groups=mesh['ep'=4,'tp'=8] {'ep'}, dimensions={0}, use_global_device_ids=true | all-gather | bytes 327680 | tf_op jit(solution)/shard_map/all_gather | solution.py:130
  84.7 0.7 gather_fusion
  85.4 2.7 %fusion.9 = f32[64,896]{1,0:T(8,128)S(1)} fusion(bf16[64,2048]{1,0:T(8,128)(2,1)S(1)} %gather_fusion, bf16[1,2048,896]{2,1,0:T(8,128)(2,1)} %param.32), kind=kOutput, calls=%fused_computation.14 | convolution fusion | flops 234881024 | bytes 4161536 | tf_op jit(solution)/shard_map/jnd,jdf->jnf/dot_general | solution.py:45
  88.2 4.7 %fusion.11 = f32[64,2048]{1,0:T(8,128)S(1)} fusion(bf16[1,896,2048]{2,1,0:T(8,128)(2,1)} %param.34, bf16[64,2048]{1,0:T(8,128)(2,1)S(1)} %gather_fusion, bf16[1,2048,896]{2,1,0:T(8,128)(2,1)} %param.33, f32[64]{0:T(128)S(1)} %mul.215, f32[64,896]{1,0:T(8,128)S(1)} %fusion.9), kind=kOutput, calls=%fused_computation.16 | convolution fusion | flops 470237184 | bytes 8356096 | tf_op jit(solution)/shard_map/jnf,jfd->jnd/dot_general | solution.py:48
  92.9 1.5 %scatter_custom_fusion = f32[65,2048]{1,0:T(8,128)S(1)} fusion(s32[64]{0:T(128)S(1)} %fusion.59, f32[64,2048]{1,0:T(8,128)S(1)} %fusion.11, f32[]{:T(128)} %constant.24.clone.1), kind=kCustom, calls=%fused_computation.28 | custom fusion | flops 131072 | bytes 532484 | tf_op jit(solution)/shard_map/scatter-add | solution.py:158
  94.5 43.9 %all-reduce.3 = bf16[64,2048]{1,0:T(8,128)(2,1)S(1)} all-reduce(f32[64,2048]{1,0:T(8,128)S(1)} %slice.20), channel_id=3, replica_groups=mesh['ep'=4,'tp'=8] {'ep','tp'}, use_global_device_ids=true, to_apply=%region_13.14.clone | all-reduce | flops 131072 | bytes 786432
  138.4 0.1 fusion.43
  138.5 0.7 fusion.46
  (59 shorter events, 1.1 us)
Async XLA Ops:
  0.0 44.6 %copy-start = (bf16[2,32,4096]{2,1,0:T(8,128)(2,1)S(1)}, bf16[2,32,4096]{2,1,0:T(8,128)(2,1)}, u32[]{:S(2)}) copy-start(bf16[2,32,4096]{2,1,0:T(8,128)(2,1)} %param.24) | copy-start | bytes 1572868
  0.0 19.9 %copy-start.1 = (bf16[16,2048]{1,0:T(8,128)(2,1)S(1)}, bf16[16,2048]{1,0:T(8,128)(2,1)}, u32[]{:S(2)}) copy-start(bf16[16,2048]{1,0:T(8,128)(2,1)} %param.18) | copy-start | bytes 196612
  0.0 19.9 %copy-start.7 = (f32[2048]{0:T(1024)S(1)}, f32[2048]{0:T(1024)}, u32[]{:S(2)}) copy-start(f32[2048]{0:T(1024)} %param.19) | copy-start | bytes 24580
  0.0 19.9 %copy-start.3 = (bf16[2048,128]{1,0:T(8,128)(2,1)S(1)}, bf16[2048,128]{1,0:T(8,128)(2,1)}, u32[]{:S(2)}) copy-start(bf16[2048,128]{1,0:T(8,128)(2,1)} %param.20) | copy-start | bytes 1572868
  0.0 20.2 %copy-start.6 = (f32[64,2]{0,1:T(2,128)S(1)}, f32[64,2]{0,1:T(2,128)}, u32[]{:S(2)}) copy-start(f32[64,2]{0,1:T(2,128)} %param.31) | copy-start | bytes 1540
  3.0 25.0 %all-to-all-start.1 = ((bf16[16,2,32]{2,1,0:T(2,128)(2,1)}), bf16[16,2,32]{2,1,0:T(2,128)(2,1)S(1)}, u32[]{:S(2)}, u32[]{:S(2)}) async-start(bf16[16,2,32]{2,1,0:T(2,128)(2,1)} %reshape.273), calls=%async_computation.1 | async-start | bytes 16384 | tf_op jit(solution)/shard_map/all_to_all | solution.py:91
  13.1 14.0 %copy-start.4 = (bf16[2,64,512]{2,1,0:T(8,128)(2,1)S(1)}, bf16[2,64,512]{2,1,0:T(8,128)(2,1)}, u32[]{:S(2)}) copy-start(bf16[2,64,512]{2,1,0:T(8,128)(2,1)} %param.22) | copy-start | bytes 393220
  28.0 10.8 %all-to-all-start = ((bf16[16,2,512]{2,1,0:T(2,128)(2,1)}), bf16[16,2,512]{2,1,0:T(2,128)(2,1)S(1)}, u32[]{:S(2)}, u32[]{:S(2)}) async-start(bf16[16,2,512]{2,1,0:T(2,128)(2,1)} %copy.39), calls=%async_computation | async-start | bytes 65536 | tf_op jit(solution)/shard_map/all_to_all | solution.py:90
  45.1 14.5 %copy-start.5 = (bf16[2,512,64]{1,2,0:T(8,128)(2,1)S(1)}, bf16[2,512,64]{1,2,0:T(8,128)(2,1)}, u32[]{:S(2)}) copy-start(bf16[2,512,64]{1,2,0:T(8,128)(2,1)} %param.26) | copy-start | bytes 393220
  45.1 14.7 %copy-start.2 = (bf16[128,2048]{1,0:T(8,128)(2,1)S(1)}, bf16[128,2048]{1,0:T(8,128)(2,1)}, u32[]{:S(2)}) copy-start(bf16[128,2048]{1,0:T(8,128)(2,1)} %param.27) | copy-start | bytes 1572868
  45.2 30.2 %copy-start.8 = (f32[2048]{0:T(1024)S(1)}, f32[2048]{0:T(1024)}, u32[]{:S(2)}) copy-start(f32[2048]{0:T(1024)} %param.28) | copy-start | bytes 24580
  45.2 30.4 %copy-start.9 = (f32[2048]{0:T(1024)S(1)}, f32[2048]{0:T(1024)}, u32[]{:S(2)}) copy-start(f32[2048]{0:T(1024)} %param.29) | copy-start | bytes 24580
  50.6 9.0 %all-to-all-start.2 = ((bf16[2,16,512]{2,0,1:T(2,128)(2,1)}), bf16[2,16,512]{2,0,1:T(2,128)(2,1)S(1)}, u32[]{:S(2)}, u32[]{:S(2)}) async-start(bf16[2,16,512]{2,0,1:T(2,128)(2,1)} %copy.42), calls=%async_computation.2 | async-start | bytes 65536 | tf_op jit(solution)/shard_map/all_to_all | solution.py:112
  88.2 50.3 %copy-start.10 = (f32[2048]{0:T(1024)S(1)}, f32[2048]{0:T(1024)}, u32[]{:S(2)}) copy-start(f32[2048]{0:T(1024)} %param.35) | copy-start | bytes 24580
